TPU v7x, 256 devices: a whole 4x4x8 slice. The times are simulated.
256 devices in a mesh: sp: 32 (over z, x), tp: 8 (over y, core).
Axes of the slice: x: 4, y: 4, z: 8, core: 2. Of those that a mesh axis runs over, the one named last changes fastest.
Arguments:
- latents: bfloat16 [16384, 2048], P(('sp', 'tp')), may hold values from -6 to 6
- context: bfloat16 [512, 2048], P('sp'), may hold values from -6 to 6
- cond: float32 [2048], P('sp'), may hold values from -6 to 6
- ctx_cond: float32 [2048], P('sp'), may hold values from -6 to 6
- mod_weight: float32 [2048, 6144], P('sp', 'tp'), may hold values from -0.125 to 0.125
- query_weight: bfloat16 [2048, 2048], P(None, 'tp'), may hold values from -1 to 1, as said below
- key_matrix: bfloat16 [2048, 1024], P(None, 'tp'), may hold values from -1 to 1, as said below
- value_matrix: bfloat16 [2048, 1024], P(None, 'tp'), may hold values from -0.125 to 0.125
- out_weight: bfloat16 [2048, 2048], P('tp'), may hold values from -0.125 to 0.125
- query_gain: float32 [128], replicated, may hold values from 0.7 to 7
- key_gain: float32 [128], replicated, may hold values from 0.7 to 7
Outputs:
- updated: bfloat16 [16384, 2048], P(('sp', 'tp'))
Inputs may be any that keep to these rules, and one draw needn't show every extreme that they name: `query_weight`: entries of order 2048 to the power -1/2. `key_matrix`: entries of order 2048 to the power -1/2.
All inputs are finite; a program needn't handle non-finite values.
Results may differ from a plain program's by a relative error of at most 0.0085.
The roundings to bfloat16 on the way count: a program that leaves them out, or rounds other values in their place, can miss the bound.
Values may be sent and summed in bfloat16 or wider, within the bound.
No kernel may reach another device: no remote copies, remote signals or barrier semaphores. Data moves between devices by JAX's collectives and lax.ppermute only.
A program may use at most 128 MiB of HBM per device.

v0:
```python
import math
import jax
import jax.numpy as jnp
from jax import lax
from jax.sharding import Mesh
from jax.sharding import PartitionSpec as P

GRID_W = 64
SP = ("sp_0", "sp_1")
SP_TP = ("sp_0", "sp_1", "tp")
NORM_EPS = 1e-06
ROPE_BASE = 10000.0


def over_axes(value, axes):
    for axis in axes:
        value = lax.psum(value, axis)
    return value


def side_by_side(arrays, axis, dim, along):
    both = jnp.concatenate(arrays, axis=along)
    filled, at, done = (lax.all_gather(both, axis, axis=dim, tiled=True), 0, [])
    for a in arrays:
        done.append(lax.slice_in_dim(filled, at, at + a.shape[along], axis=along))
        at += a.shape[along]
    return tuple(done)


def normalize(latent_value_rows):
    return latent_value_rows * lax.rsqrt(
        jnp.mean(latent_value_rows * latent_value_rows, axis=-1, keepdims=True) + NORM_EPS
    )


def rotate(latent_value_rows, positions):
    quarter = latent_value_rows.shape[-1] // 2
    inv_freq = ROPE_BASE ** (-jnp.arange(quarter, dtype=jnp.float32) / quarter)
    angles = positions.astype(jnp.float32)[:, None] * inv_freq[None, :]
    cos_table = jnp.cos(angles)[:, None, :]
    sin_table = jnp.sin(angles)[:, None, :]
    first, second = (latent_value_rows[..., :quarter], latent_value_rows[..., quarter:])
    return jnp.concatenate(
        [first * cos_table - second * sin_table, second * cos_table + first * sin_table], axis=-1
    )


def axial(latent_value_rows, positions):
    half_dim = latent_value_rows.shape[-1] // 2
    return jnp.concatenate(
        [
            rotate(latent_value_rows[..., :half_dim], positions // GRID_W),
            rotate(latent_value_rows[..., half_dim:], positions % GRID_W),
        ],
        axis=-1,
    )


def modulate(latent_value_rows, mod_row):
    model_width = latent_value_rows.shape[-1]
    shift_vec = mod_row[:model_width]
    scale_vec = mod_row[model_width : 2 * model_width]
    return (
        normalize(latent_value_rows.astype(jnp.float32)) * (1.0 + scale_vec) + shift_vec
    ).astype(jnp.bfloat16)


def body(
    latents,
    context,
    cond,
    ctx_cond,
    mod_weight,
    query_weight,
    key_matrix,
    value_matrix,
    out_weight,
    query_gain,
    key_gain,
):
    model_width = latents.shape[1]
    head_dim = query_gain.shape[0]
    sp_count = lax.axis_size(SP)
    partials = jnp.dot(
        jax.nn.silu(jnp.stack([cond, ctx_cond])), mod_weight, precision=lax.Precision.HIGHEST
    )
    summed = over_axes(partials, SP)
    modulation = lax.all_gather(summed, "tp", axis=1, tiled=True)
    gate_vec = modulation[0, 2 * model_width :]
    normalised_rows = modulate(latents, modulation[0])
    prefix_normalised = modulate(context, modulation[1])
    query_cols = query_weight.shape[1]
    key_cols = key_matrix.shape[1]
    piece = lax.all_gather(normalised_rows, "tp", axis=0, tiled=True)
    projected = jnp.concatenate(
        [
            jnp.dot(piece, query_weight, preferred_element_type=jnp.float32),
            jnp.dot(piece, key_matrix, preferred_element_type=jnp.float32),
            jnp.dot(piece, value_matrix, preferred_element_type=jnp.float32),
        ],
        axis=1,
    )
    row_count = projected.shape[0]
    positions = lax.axis_index(SP) * row_count + jnp.arange(row_count, dtype=jnp.int32)
    query_heads = projected[:, :query_cols].reshape(row_count, -1, head_dim)
    query_heads = axial(normalize(query_heads) * query_gain, positions).astype(jnp.bfloat16)
    key_heads = projected[:, query_cols : query_cols + key_cols].reshape(row_count, -1, head_dim)
    key_heads = axial(normalize(key_heads) * key_gain, positions).astype(jnp.bfloat16)
    value_heads = (
        projected[:, query_cols + key_cols :].reshape(row_count, -1, head_dim).astype(jnp.bfloat16)
    )
    key_part = jnp.dot(prefix_normalised, key_matrix, preferred_element_type=jnp.float32).reshape(
        prefix_normalised.shape[0], -1, head_dim
    )
    value_part = jnp.dot(
        prefix_normalised, value_matrix, preferred_element_type=jnp.float32
    ).reshape(prefix_normalised.shape[0], -1, head_dim)
    local_keys = (normalize(key_part) * key_gain).astype(jnp.bfloat16)
    local_values = value_part.astype(jnp.bfloat16)
    prefix_keys, prefix_values = side_by_side((local_keys, local_values), SP, 0, 1)
    kv_local = key_heads.shape[1]
    group_size = query_heads.shape[1] // kv_local
    grouped = query_heads.reshape(row_count, kv_local, group_size, head_dim).transpose(1, 2, 0, 3)
    grouped = grouped.reshape(kv_local, group_size * row_count, head_dim)
    inv_root = head_dim ** (-0.5)
    lift = math.log(sp_count * row_count / (2.0 * prefix_keys.shape[0]))
    ctx_scores = (
        jnp.einsum("hqd,khd->hqk", grouped, prefix_keys, preferred_element_type=jnp.float32)
        * inv_root
        + lift
    )
    top_init = jnp.max(ctx_scores, axis=-1)
    ctx_weights = jnp.exp(ctx_scores - top_init[..., None])
    initial = (
        top_init,
        jnp.sum(ctx_weights, axis=-1),
        jnp.einsum(
            "hqk,khd->hqd",
            ctx_weights.astype(jnp.bfloat16),
            prefix_values,
            preferred_element_type=jnp.float32,
        ),
    )

    def update(state_now, key_block, value_block):
        top_old, total_old, acc_old = state_now
        scores = (
            jnp.einsum("hqd,khd->hqk", grouped, key_block, preferred_element_type=jnp.float32)
            * inv_root
        )
        top_new = jnp.maximum(top_old, jnp.max(scores, axis=-1))
        factor = jnp.exp(top_old - top_new)
        weights_now = jnp.exp(scores - top_new[..., None])
        acc_new = acc_old * factor[..., None] + jnp.einsum(
            "hqk,khd->hqd",
            weights_now.astype(jnp.bfloat16),
            value_block,
            preferred_element_type=jnp.float32,
        )
        return (top_new, total_old * factor + jnp.sum(weights_now, axis=-1), acc_new)

    key_piece, value_piece = side_by_side((key_heads, value_heads), SP, 0, 1)
    key_count = key_piece.shape[0]
    rows_per_block = math.gcd(key_count, 2048)
    block_count = key_count // rows_per_block
    key_blocks = key_piece.reshape(block_count, rows_per_block, kv_local, head_dim)
    value_blocks = value_piece.reshape(block_count, rows_per_block, kv_local, head_dim)

    def one_step(state_in, blocks_in):
        return (update(state_in, blocks_in[0], blocks_in[1]), None)

    state_out, _ = lax.scan(one_step, initial, (key_blocks, value_blocks))
    top_fin, total_fin, acc_fin = state_out
    attended = (acc_fin / total_fin[..., None]).astype(jnp.bfloat16)
    attended = (
        attended.reshape(kv_local, group_size, row_count, head_dim)
        .transpose(2, 0, 1, 3)
        .reshape(row_count, -1)
    )
    exchanged = lax.all_to_all(attended, "tp", split_axis=0, concat_axis=1, tiled=True)
    mixed_rows = jnp.dot(
        exchanged,
        lax.all_gather(out_weight, "tp", axis=0, tiled=True),
        preferred_element_type=jnp.float32,
    )
    return (latents.astype(jnp.float32) + gate_vec * normalize(mixed_rows)).astype(jnp.bfloat16)


def solution(mesh):
    torus = Mesh(mesh.devices.reshape(8, 4, mesh.shape["tp"]), ("sp_0", "sp_1", "tp"))
    placed = (
        P(SP_TP, None),
        P(SP, None),
        P(SP),
        P(SP),
        P(SP, "tp"),
        P(None, "tp"),
        P(None, "tp"),
        P(None, "tp"),
        P("tp", None),
        P(),
        P(),
    )
    return jax.shard_map(
        body, mesh=torus, in_specs=placed, out_specs=P(SP_TP, None), check_vma=False
    )
```

profile of v0, /device:TPU:1, one launch (start us, length us, event | category | flops | bytes accessed | tf_op | source)
XLA Modules:
  0.0 285.0 jit_solution(6609689054624795851)
XLA Ops:
  7.8 17.5 %psum.14 = f32[2,768]{1,0:T(2,128)S(1)} all-reduce(f32[2,768]{1,0:T(2,128)S(1)} %fusion.67), channel_id=1, replica_groups=mesh['sp_0'=8,'sp_1'=4,'tp'=8] {'sp_0'}, use_global_device_ids=true, to_apply=%region_0.1 | all-reduce | flops 1536 | bytes 12288 | tf_op jit(solution)/shard_map/psum | solution.py:17
  25.3 8.6 %psum.15 = f32[2,768]{1,0:T(2,128)S(1)} all-reduce(f32[2,768]{1,0:T(2,128)S(1)} %psum.14), channel_id=1, replica_groups=mesh['sp_0'=8,'sp_1'=4,'tp'=8] {'sp_1'}, use_global_device_ids=true, to_apply=%region_1.2 | all-reduce | flops 1536 | bytes 12288 | tf_op jit(solution)/shard_map/psum | solution.py:17
  33.9 19.5 %all_gather.15 = f32[2,6144]{1,0:T(2,128)S(1)} all-gather(f32[2,768]{1,0:T(2,128)S(1)} %psum.15), channel_id=1, replica_groups=mesh['sp_0'=8,'sp_1'=4,'tp'=8] {'tp'}, dimensions={1}, use_global_device_ids=true | all-gather | bytes 55296 | tf_op jit(solution)/shard_map/all_gather | solution.py:88
  56.5 23.1 %all-gather.4.cloned.1.call-done = bf16[512,2048]{1,0:T(8,128)(2,1)} async-done(((bf16[64,2048]{1,0:T(8,128)(2,1)}), bf16[512,2048]{1,0:T(8,128)(2,1)}) %all-gather.4.cloned.1.call-update) | async-done | bytes 2097168 | tf_op jit(solution)/shard_map/all_gather | solution.py:94
  79.5 2.5 multiply_reduce_fusion.3
  82.7 2.5 fusion.22
  86.8 3.0 %multiply_cosine_fusion.1 = (f32[512,32]{1,0:T(8,128)S(1)}, f32[512,32]{1,0:T(8,128)}, f32[512,32]{1,0:T(8,128)}, f32[512,32]{1,0:T(8,128)}) fusion(f32[32]{0:T(128)S(1)} %multiply_power_fusion, f32[512]{0:T(512)S(1)} %get-tuple-element.112, f32[512]{0:T(512)S(1)} %get-tuple-element.113), kind=kLoop, calls=%fused_computation.50 | loop fusion | flops 32768 | bytes 266368 | tf_op jit(solution)/shard_map/cos | solution.py:40
  92.6 40.4 %all_gather.17 = bf16[512,2,128]{2,0,1:T(8,128)(2,1)} all-gather(bf16[16,2,128]{2,0,1:T(8,128)(2,1)S(1)} %pad_maximum_fusion.2), channel_id=1, replica_groups=mesh['sp_0'=8,'sp_1'=4,'tp'=8] {'sp_0','sp_1'}, dimensions={0}, use_global_device_ids=true | all-gather | bytes 270336 | tf_op jit(solution)/shard_map/all_gather | solution.py:23
  139.6 46.4 %all-gather.6.cloned.1.call-done = bf16[16384,2,128]{0,2,1:T(8,128)(2,1)} async-done(((bf16[512,2,128]{0,2,1:T(8,128)(2,1)}), bf16[16384,2,128]{0,2,1:T(8,128)(2,1)}) %all-gather.6.cloned.1.call-update) | async-done | bytes 8388624 | tf_op jit(solution)/shard_map/all_gather | solution.py:23
  186.1 5.8 %fusion.76 = (bf16[16384,1,128]{0,2,1:T(8,128)(2,1)}, bf16[16384,1,128]{0,2,1:T(8,128)(2,1)}) fusion(bf16[16384,2,128]{0,2,1:T(8,128)(2,1)} %all-gather.6.cloned.1.call-done), kind=kLoop, calls=%fused_computation.126 | loop fusion | bytes 16777216 | tf_op jit(solution)/shard_map/slice | solution.py:25
  191.9 6.3 %copy.23 = bf16[16384,1,128]{2,0,1:T(8,128)(2,1)} copy(bf16[16384,1,128]{0,2,1:T(8,128)(2,1)} %get-tuple-element.78) | data formatting | bytes 8388608 | tf_op jit(solution)/shard_map/while | solution.py:172
  198.2 6.5 %copy.24 = bf16[16384,1,128]{2,0,1:T(8,128)(2,1)} copy(bf16[16384,1,128]{0,2,1:T(8,128)(2,1)} %get-tuple-element.77) | data formatting | bytes 8388608 | tf_op jit(solution)/shard_map/while | solution.py:172
  204.7 52.6 %while.14 = (s32[]{:T(128)}, f32[1,1024]{1,0:T(1,128)S(1)}, f32[1,1024]{1,0:T(1,128)S(1)}, f32[1,1024,128]{2,1,0:T(8,128)S(1)}, bf16[8,2048,1,128]{3,1,2,0:T(8,1...) while((s32[]{:T(128)}, f32[1,1024]{1,0:T(1,128)S(1)}, ...), condition=%wide.region_12.13_spmd, body=%wide.region_9.12_spmd.sunk | while | flops 1090783232 | bytes 27590756 | solution.py:172
  204.7 2.3 multiply_reduce_fusion.6
  208.5 2.8 fusion.97
  215.1 2.8 fusion.97
  221.6 2.8 fusion.97
  228.2 2.8 fusion.97
  234.8 2.8 fusion.97
  241.4 2.8 fusion.97
  247.9 2.8 fusion.97
  254.5 2.8 fusion.97
  258.0 14.5 %all_to_all.19 = bf16[8,64,256]{2,1,0:T(8,128)(2,1)S(1)} all-to-all(bf16[8,64,256]{2,1,0:T(8,128)(2,1)S(1)} %all_to_all.14), channel_id=1, replica_groups=mesh['sp_0'=8,'sp_1'=4,'tp'=8] {'tp'}, dimensions={0} | all-to-all | bytes 524288 | tf_op jit(solution)/shard_map/all_to_all | solution.py:180
  272.5 5.1 %multiply_reduce_fusion.1 = (f32[64]{0:T(128)S(1)}, f32[64,2048]{1,0:T(8,128)S(1)}) fusion(bf16[64,2048]{1,0:T(8,128)(2,1)S(1)} %bitcast.110, bf16[2048,2048]{1,0:T(8,128)(2,1)} %all-gather.8.cloned.1.call-done), kind=kOutput, calls=%fused_computation.39 | convolution fusion | flops 537132992 | bytes 9175296 | tf_op jit(solution)/shard_map/dot_general | solution.py:181
  (93 shorter events, 45.2 us)
Async XLA Ops:
  6.5 126.6 %copy-start = (bf16[2048,256]{1,0:T(8,128)(2,1)S(1)}, bf16[2048,256]{1,0:T(8,128)(2,1)}, u32[]{:S(2)}) copy-start(bf16[2048,256]{1,0:T(8,128)(2,1)} %param.18) | copy-start | bytes 3145732
  6.5 75.5 %copy-start.5 = (f32[128]{0:T(128)S(1)}, f32[128]{0:T(128)}, u32[]{:S(2)}) copy-start(f32[128]{0:T(128)} %param.23) | copy-start | bytes 1540
  6.5 73.0 %all-gather.4.cloned.1.call-start = ((), (), s32[]{:S(2)}) async-start(), calls=%async_computation.1 | async-start | bytes 2359296 | tf_op jit(solution)/shard_map/all_gather | solution.py:94
  56.4 129.7 %all-gather.6.cloned.1.call-start = ((), (), s32[]{:S(2)}) async-start(), calls=%async_computation.2 | async-start | bytes 8650752 | tf_op jit(solution)/shard_map/all_gather | solution.py:23
  56.4 33.3 %copy-start.4 = (bf16[16,2048]{1,0:T(8,128)(2,1)S(1)}, bf16[16,2048]{1,0:T(8,128)(2,1)}, u32[]{:S(2)}) copy-start(bf16[16,2048]{1,0:T(8,128)(2,1)} %param.14) | copy-start | bytes 196612
  82.1 51.0 %copy-start.1 = (bf16[512,2048]{1,0:T(8,128)(2,1)S(1)}, bf16[512,2048]{1,0:T(8,128)(2,1)}, u32[]{:S(2)}) copy-start(bf16[512,2048]{1,0:T(8,128)(2,1)} %all-gather.4.cloned.1.call-done) | copy-start | bytes 6291460
  86.0 49.9 %copy-start.6 = (f32[128]{0:T(128)S(1)}, f32[128]{0:T(128)}, u32[]{:S(2)}) copy-start(f32[128]{0:T(128)} %param.22) | copy-start | bytes 1540
  86.0 186.5 %all-gather.8.cloned.1.call-start = ((), (), s32[]{:S(2)}) async-start(), calls=%async_computation.3 | async-start | bytes 9437184 | tf_op jit(solution)/shard_map/all_gather | solution.py:183
  134.7 3.5 %copy-start.3 = (bf16[512,2,128]{2,0,1:T(8,128)(2,1)S(1)}, bf16[512,2,128]{2,0,1:T(8,128)(2,1)}, u32[]{:S(2)}) copy-start(bf16[512,2,128]{2,0,1:T(8,128)(2,1)} %all_gather.17) | copy-start | bytes 786436
  272.5 5.1 %copy-start.2 = (bf16[64,2048]{1,0:T(8,128)(2,1)S(1)}, bf16[64,2048]{1,0:T(8,128)(2,1)}, u32[]{:S(2)}) copy-start(bf16[64,2048]{1,0:T(8,128)(2,1)} %param.13) | copy-start | bytes 786436
Sparse Core Ops, SparseCore 0:
  56.5 23.0 all-gather.3
  86.1 99.8 all-gather.5
  187.9 54.6 all-gather.7
where the time goes:
time: 286 us; the launch traced here: 285 us
  blocking collectives  100 us (35%)
  waiting for transfers between devices  70.3 us (25%)
  matrix products  57.2 us (20%)
  other arithmetic  22.9 us (8%)
  local copies, waits for them, and re-layouts  20.4 us (7%)
  between operations  13.4 us (5%)
    all_gather x1, waiting for transfers between devices, side_by_side(): filled, at, done = (lax.all_gather(both, axis, axis=dim, tiled=True), 0, [])  46.4 us
    all_gather x1, blocking collectives, side_by_side(): filled, at, done = (lax.all_gather(both, axis, axis=dim, tiled=True), 0, [])  40.4 us
    psum x2, blocking collectives, over_axes(): value = lax.psum(value, axis)  26.1 us
    all_gather x1, waiting for transfers between devices, body(): piece = lax.all_gather(normalised_rows, 'tp', axis=0, tiled=True)  23.1 us
    dot_general x8, matrix products, update(): jnp.einsum('hqk,khd->hqd', weights_now.astype(jnp.bfloat16), value_block,...  22.2 us
    all_gather x1, blocking collectives, body(): modulation = lax.all_gather(summed, 'tp', axis=1, tiled=True)  19.5 us
    dot_general x8, matrix products, update(): jnp.einsum('hqd,khd->hqk', grouped, key_block, preferred_element_type=jnp...  18.4 us
    all_to_all x1, blocking collectives, body(): lax.all_to_all(attended, 'tp', split_axis=0, concat_axis=1, tiled=True)  14.5 us
  transfers between devices with their start and end apart: 3, of which 2 were waited for; matrix products, arithmetic and copies ran while one was open for 29% of the time, Pallas kernels for 0%

commit v1 on v0

--- a/solution.py
+++ b/solution.py
@@ -177,7 +177,10 @@
         .transpose(2, 0, 1, 3)
         .reshape(row_count, -1)
     )
-    exchanged = lax.all_to_all(attended, "tp", split_axis=0, concat_axis=1, tiled=True)
+    exchanged = jnp.concatenate(
+        lax.all_to_all(jnp.stack(jnp.split(attended, lax.axis_size("tp"), axis=0)), "tp", 0, 0),
+        axis=1,
+    )
     mixed_rows = jnp.dot(
         exchanged,
         lax.all_gather(out_weight, "tp", axis=0, tiled=True),

time: 286 us -> 287 us (level)
  transfers between devices with their start and end apart: 3 -> 3, of which waited for: 2 -> 2; matrix products, arithmetic and copies ran while one was open for 29% -> 30% of each run, Pallas kernels for 0% -> 0%
where the time goes in v1:
time: 287 us; the launch traced here: 285 us
  blocking collectives  100 us (35%)
  waiting for transfers between devices  70.2 us (24%)
  matrix products  57.2 us (20%)
  other arithmetic  22.9 us (8%)
  local copies, waits for them, and re-layouts  20.7 us (7%)
  between operations  13.5 us (5%)
    all_gather x1, waiting for transfers between devices, side_by_side(): filled, at, done = (lax.all_gather(both, axis, axis=dim, tiled=True), 0, [])  46.4 us
    all_gather x1, blocking collectives, side_by_side(): filled, at, done = (lax.all_gather(both, axis, axis=dim, tiled=True), 0, [])  40.4 us
    psum x2, blocking collectives, over_axes(): value = lax.psum(value, axis)  26.1 us
    all_gather x1, waiting for transfers between devices, body(): piece = lax.all_gather(normalised_rows, 'tp', axis=0, tiled=True)  23.1 us
    dot_general x8, matrix products, update(): jnp.einsum('hqk,khd->hqd', weights_now.astype(jnp.bfloat16), value_block,...  22.2 us
    all_gather x1, blocking collectives, body(): modulation = lax.all_gather(summed, 'tp', axis=1, tiled=True)  19.5 us
    dot_general x8, matrix products, update(): jnp.einsum('hqd,khd->hqk', grouped, key_block, preferred_element_type=jnp...  18.4 us
    all_to_all x1, blocking collectives, body(): lax.all_to_all(jnp.stack(jnp.split(attended, lax.axis_size('tp'), axis=0)...  14.5 us
  transfers between devices with their start and end apart: 3, of which 2 were waited for; matrix products, arithmetic and copies ran while one was open for 30% of the time, Pallas kernels for 0%

profile of v1, /device:TPU:1, one launch (start us, length us, event | category | flops | bytes accessed | tf_op | source)
XLA Modules:
  0.0 285.4 jit_solution(9054854437950963230)
XLA Ops:
  7.8 17.5 %psum.14 = f32[2,768]{1,0:T(2,128)S(1)} all-reduce(f32[2,768]{1,0:T(2,128)S(1)} %fusion.67), channel_id=1, replica_groups=mesh['sp_0'=8,'sp_1'=4,'tp'=8] {'sp_0'}, use_global_device_ids=true, to_apply=%region_0.1 | all-reduce | flops 1536 | bytes 12288 | tf_op jit(solution)/shard_map/psum | solution.py:17
  25.3 8.6 %psum.15 = f32[2,768]{1,0:T(2,128)S(1)} all-reduce(f32[2,768]{1,0:T(2,128)S(1)} %psum.14), channel_id=1, replica_groups=mesh['sp_0'=8,'sp_1'=4,'tp'=8] {'sp_1'}, use_global_device_ids=true, to_apply=%region_1.2 | all-reduce | flops 1536 | bytes 12288 | tf_op jit(solution)/shard_map/psum | solution.py:17
  33.9 19.5 %all_gather.15 = f32[2,6144]{1,0:T(2,128)S(1)} all-gather(f32[2,768]{1,0:T(2,128)S(1)} %psum.15), channel_id=1, replica_groups=mesh['sp_0'=8,'sp_1'=4,'tp'=8] {'tp'}, dimensions={1}, use_global_device_ids=true | all-gather | bytes 55296 | tf_op jit(solution)/shard_map/all_gather | solution.py:88
  56.5 23.1 %all-gather.4.cloned.1.call-done = bf16[512,2048]{1,0:T(8,128)(2,1)} async-done(((bf16[64,2048]{1,0:T(8,128)(2,1)}), bf16[512,2048]{1,0:T(8,128)(2,1)}) %all-gather.4.cloned.1.call-update) | async-done | bytes 2097168 | tf_op jit(solution)/shard_map/all_gather | solution.py:94
  79.5 2.5 multiply_reduce_fusion.3
  82.7 2.5 fusion.22
  86.8 3.0 %multiply_cosine_fusion.1 = (f32[512,32]{1,0:T(8,128)S(1)}, f32[512,32]{1,0:T(8,128)}, f32[512,32]{1,0:T(8,128)}, f32[512,32]{1,0:T(8,128)}) fusion(f32[32]{0:T(128)S(1)} %multiply_power_fusion, f32[512]{0:T(512)S(1)} %get-tuple-element.120, f32[512]{0:T(512)S(1)} %get-tuple-element.121), kind=kLoop, calls=%fused_computation.50 | loop fusion | flops 32768 | bytes 266368 | tf_op jit(solution)/shard_map/cos | solution.py:40
  92.6 40.4 %all_gather.17 = bf16[512,2,128]{2,0,1:T(8,128)(2,1)} all-gather(bf16[16,2,128]{2,0,1:T(8,128)(2,1)S(1)} %pad_maximum_fusion.2), channel_id=1, replica_groups=mesh['sp_0'=8,'sp_1'=4,'tp'=8] {'sp_0','sp_1'}, dimensions={0}, use_global_device_ids=true | all-gather | bytes 270336 | tf_op jit(solution)/shard_map/all_gather | solution.py:23
  139.6 46.4 %all-gather.6.cloned.1.call-done = bf16[16384,2,128]{0,2,1:T(8,128)(2,1)} async-done(((bf16[512,2,128]{0,2,1:T(8,128)(2,1)}), bf16[16384,2,128]{0,2,1:T(8,128)(2,1)}) %all-gather.6.cloned.1.call-update) | async-done | bytes 8388624 | tf_op jit(solution)/shard_map/all_gather | solution.py:23
  186.1 5.8 %fusion.76 = (bf16[16384,1,128]{0,2,1:T(8,128)(2,1)}, bf16[16384,1,128]{0,2,1:T(8,128)(2,1)}) fusion(bf16[16384,2,128]{0,2,1:T(8,128)(2,1)} %all-gather.6.cloned.1.call-done), kind=kLoop, calls=%fused_computation.134 | loop fusion | bytes 16777216 | tf_op jit(solution)/shard_map/slice | solution.py:25
  191.9 6.3 %copy.23 = bf16[16384,1,128]{2,0,1:T(8,128)(2,1)} copy(bf16[16384,1,128]{0,2,1:T(8,128)(2,1)} %get-tuple-element.78) | data formatting | bytes 8388608 | tf_op jit(solution)/shard_map/while | solution.py:172
  198.2 6.5 %copy.24 = bf16[16384,1,128]{2,0,1:T(8,128)(2,1)} copy(bf16[16384,1,128]{0,2,1:T(8,128)(2,1)} %get-tuple-element.77) | data formatting | bytes 8388608 | tf_op jit(solution)/shard_map/while | solution.py:172
  204.7 52.6 %while.14 = (s32[]{:T(128)}, f32[1,1024]{1,0:T(1,128)S(1)}, f32[1,1024]{1,0:T(1,128)S(1)}, f32[1,1024,128]{2,1,0:T(8,128)S(1)}, bf16[8,2048,1,128]{3,1,2,0:T(8,1...) while((s32[]{:T(128)}, f32[1,1024]{1,0:T(1,128)S(1)}, ...), condition=%wide.region_12.13_spmd, body=%wide.region_9.12_spmd.sunk | while | flops 1090783232 | bytes 27591764 | solution.py:172
  204.7 2.3 multiply_reduce_fusion.6
  208.5 2.8 fusion.98
  215.1 2.8 fusion.98
  221.6 2.8 fusion.98
  228.2 2.8 fusion.98
  234.8 2.8 fusion.98
  241.4 2.8 fusion.98
  247.9 2.8 fusion.98
  254.5 2.8 fusion.98
  258.3 14.5 %all_to_all.5 = bf16[8,64,256]{2,1,0:T(8,128)(2,1)S(1)} all-to-all(bf16[8,64,256]{2,1,0:T(8,128)(2,1)S(1)} %constant_dynamic-update-slice_fusion), channel_id=1, replica_groups=mesh['sp_0'=8,'sp_1'=4,'tp'=8] {'tp'}, dimensions={0} | all-to-all | bytes 524288 | tf_op jit(solution)/shard_map/all_to_all | solution.py:181
  272.9 5.1 %multiply_reduce_fusion.1 = (f32[64]{0:T(128)S(1)}, f32[64,2048]{1,0:T(8,128)S(1)}) fusion(bf16[64,2048]{1,0:T(8,128)(2,1)S(1)} %bitcast.124, bf16[2048,2048]{1,0:T(8,128)(2,1)} %all-gather.8.cloned.1.call-done), kind=kOutput, calls=%fused_computation.39 | convolution fusion | flops 537132992 | bytes 9175296 | tf_op jit(solution)/shard_map/dot_general | solution.py:184
  (109 shorter events, 45.4 us)
Async XLA Ops:
  6.5 126.6 %copy-start = (bf16[2048,256]{1,0:T(8,128)(2,1)S(1)}, bf16[2048,256]{1,0:T(8,128)(2,1)}, u32[]{:S(2)}) copy-start(bf16[2048,256]{1,0:T(8,128)(2,1)} %param.18) | copy-start | bytes 3145732
  6.5 75.5 %copy-start.5 = (f32[128]{0:T(128)S(1)}, f32[128]{0:T(128)}, u32[]{:S(2)}) copy-start(f32[128]{0:T(128)} %param.23) | copy-start | bytes 1540
  6.5 73.0 %all-gather.4.cloned.1.call-start = ((), (), s32[]{:S(2)}) async-start(), calls=%async_computation.1 | async-start | bytes 2359296 | tf_op jit(solution)/shard_map/all_gather | solution.py:94
  56.4 129.7 %all-gather.6.cloned.1.call-start = ((), (), s32[]{:S(2)}) async-start(), calls=%async_computation.2 | async-start | bytes 8650752 | tf_op jit(solution)/shard_map/all_gather | solution.py:23
  56.4 33.3 %copy-start.4 = (bf16[16,2048]{1,0:T(8,128)(2,1)S(1)}, bf16[16,2048]{1,0:T(8,128)(2,1)}, u32[]{:S(2)}) copy-start(bf16[16,2048]{1,0:T(8,128)(2,1)} %param.14) | copy-start | bytes 196612
  82.1 51.0 %copy-start.1 = (bf16[512,2048]{1,0:T(8,128)(2,1)S(1)}, bf16[512,2048]{1,0:T(8,128)(2,1)}, u32[]{:S(2)}) copy-start(bf16[512,2048]{1,0:T(8,128)(2,1)} %all-gather.4.cloned.1.call-done) | copy-start | bytes 6291460
  86.0 49.9 %copy-start.6 = (f32[128]{0:T(128)S(1)}, f32[128]{0:T(128)}, u32[]{:S(2)}) copy-start(f32[128]{0:T(128)} %param.22) | copy-start | bytes 1540
  86.0 186.8 %all-gather.8.cloned.1.call-start = ((), (), s32[]{:S(2)}) async-start(), calls=%async_computation.3 | async-start | bytes 9437184 | tf_op jit(solution)/shard_map/all_gather | solution.py:186
  134.7 3.5 %copy-start.3 = (bf16[512,2,128]{2,0,1:T(8,128)(2,1)S(1)}, bf16[512,2,128]{2,0,1:T(8,128)(2,1)}, u32[]{:S(2)}) copy-start(bf16[512,2,128]{2,0,1:T(8,128)(2,1)} %all_gather.17) | copy-start | bytes 786436
  272.9 5.1 %copy-start.2 = (bf16[64,2048]{1,0:T(8,128)(2,1)S(1)}, bf16[64,2048]{1,0:T(8,128)(2,1)}, u32[]{:S(2)}) copy-start(bf16[64,2048]{1,0:T(8,128)(2,1)} %param.13) | copy-start | bytes 786436
Sparse Core Ops, SparseCore 0:
  56.5 23.0 all-gather.3
  86.1 99.8 all-gather.5
  187.9 54.6 all-gather.7
